TPU v7x, 512 devices: a whole 4x4x16 slice. The times are simulated.
512 devices in a mesh: kv: 16 (over y, x), tp: 32 (over z, core).
Axes of the slice: x: 4, y: 4, z: 16, core: 2. Of those that a mesh axis runs over, the one named last changes fastest.
Arguments:
- tokens: bfloat16 [3, 4096], P(None, ('kv', 'tp')), may hold values from -40 to 40
- lengths: int32 [3], replicated, may hold values from 1 to 131072, as said below
- attn_gain: float32 [4096], P(('kv', 'tp')), may hold values from 0.1 to 1.9
- w_query: bfloat16 [4096, 2048], P('kv', 'tp'), may hold values from -0.09375 to 0.09375
- w_key: bfloat16 [4096, 128], P('kv'), may hold values from -0.09375 to 0.09375
- w_value: bfloat16 [4096, 128], P('kv'), may hold values from -0.09375 to 0.09375
- w_forget: bfloat16 [4096, 32], replicated, may hold values from -0.09375 to 0.09375
- forget_bias: float32 [32], replicated, may hold values from -4 to 0
- cache_keys: bfloat16 [3, 128, 131072], P(None, None, ('kv', 'tp')), may hold values from -320 to 320
- cache_values: bfloat16 [3, 128, 131072], P(None, None, ('kv', 'tp')), may hold values from -6 to 6
- cache_decay: float32 [3, 32, 131072], P(None, None, ('kv', 'tp')), may hold values from -16388 to 0, as said below
- out_gain: float32 [2048], replicated, may hold values from 0.1 to 1.9
- w_out: bfloat16 [2048, 4096], P('tp', 'kv'), may hold values from -0.125 to 0.125
- mlp_gain: float32 [4096], P(('kv', 'tp')), may hold values from 0.1 to 1.9
- w_gate: bfloat16 [4096, 11264], P('kv', 'tp'), may hold values from -0.09375 to 0.09375
- w_up: bfloat16 [4096, 11264], P('kv', 'tp'), may hold values from -0.09375 to 0.09375
- w_down: bfloat16 [11264, 4096], P('tp', 'kv'), may hold values from -0.0546875 to 0.0546875
Outputs:
- layer_out: bfloat16 [3, 4096], P(None, ('kv', 'tp'))
Inputs may be any that keep to these rules, and one draw needn't show every extreme that they name: Sequence b has lengths[b] live cache positions, 0 to lengths[b] - 1; some sequence has exactly 131072 in every draw. On live positions, cache_decay[b, h, j] is the sum of the log forget gates of sequence b and head h over positions j + 1 to lengths[b] - 1, so it is zero at the last live position and never rises toward earlier positions; it is zero beyond lengths[b].
All inputs are finite; a program needn't handle non-finite values.
Results may differ from a plain program's by a relative error of at most 0.013.
Values may be sent and summed in bfloat16 or wider, within the bound.
A program may use at most 64 MiB of HBM per device.

v0:
```python
import jax
import jax.numpy as jnp
from jax import lax
from jax.sharding import Mesh
from jax.sharding import PartitionSpec as P

QUERY_HEAD_COUNT = 32
HD = 64
KV_HEADS = 2
TP = ("tp_0", "tp_1")
KV = ("kv_0", "kv_1")
KV_TP = ("kv_0", "kv_1", "tp_0", "tp_1")
epsilon = 1e-06
masked_score = -1e30


def sent_to_all(x, axis):
    copies = jnp.broadcast_to(x, (lax.axis_size(axis), *x.shape))
    return lax.all_to_all(copies, axis, split_axis=0, concat_axis=0, tiled=True)


def joined_along(blocks, dim):
    lengths = list(blocks.shape[1:])
    lengths[dim] *= blocks.shape[0]
    return jnp.moveaxis(blocks, 0, dim).reshape(lengths)


def collect(x, axis, dim):
    blocks = sent_to_all(x, axis)
    return joined_along(blocks, dim)


def by_axis(x, axes):
    for axis in axes:
        x = lax.psum(x, axis)
    return x


def all_in_one(x, axis):
    leaves = jax.tree.leaves(x)
    turns = sorted(range(len(leaves)), key=lambda k: -leaves[k].size)
    width = (1, *leaves[turns[0]].shape)[-1]
    lines = [
        jnp.pad(leaves[k].reshape(-1), (0, -leaves[k].size % width)).reshape(-1, width)
        for k in turns
    ]
    both, at, found = (lax.all_gather(jnp.concatenate(lines), axis), 0, {})
    for k, line in zip(turns, lines):
        piece = both[:, at : at + len(line)].reshape(len(both), -1)
        found[k] = piece[:, : leaves[k].size].reshape(-1, *leaves[k].shape)
        at += len(line)
    numbers = iter(range(len(leaves)))
    return jax.tree.map(lambda _: found[next(numbers)], x)


def merged_by_axis(x, axes, combine):
    for axis in axes:
        pieces = all_in_one(x, axis)
        x = jax.tree.map(lambda part: part[0], pieces)
        for k in range(1, lax.axis_size(axis)):
            x = combine(x, jax.tree.map(lambda part: part[k], pieces))
    return x


def in_blocks(x, dim, length):
    lengths = x.shape
    blocks = x.reshape(*lengths[:dim], length, lengths[dim] // length, *lengths[dim + 1 :])
    return jnp.moveaxis(blocks, dim, 0)


def summed_on_arrival(x, axis, dim):
    length = lax.axis_size(axis)
    blocks = lax.all_to_all(in_blocks(x, dim, length), axis, 0, 0, tiled=True)
    return jnp.sum(blocks, axis=0)


def spread_rows(share, gain):
    scaled = (share.astype(jnp.float32) * gain).astype(jnp.bfloat16)
    squares = jnp.sum(jnp.square(share.astype(jnp.float32)), axis=1)
    row_block, square_parts = (
        collect(scaled.astype(jnp.float32), TP, 1).astype(scaled.dtype),
        collect(squares[:, None], TP, 1),
    )
    square_total = jnp.sum(square_parts, axis=1)
    return (row_block, square_total)


def combine_partials(earlier, later):
    top_a, total_a, sums_a = earlier
    top_b, total_b, sums_b = later
    score_top = jnp.maximum(top_a, top_b)
    scale_a = jnp.exp(top_a - score_top)
    scale_b = jnp.exp(top_b - score_top)
    return (
        score_top,
        total_a * scale_a + total_b * scale_b,
        sums_a * scale_a[..., None] + sums_b * scale_b[..., None],
    )


def body(
    tokens,
    lengths,
    attn_gain,
    w_query,
    w_key,
    w_value,
    w_forget,
    forget_bias,
    cache_keys,
    cache_values,
    cache_decay,
    out_gain,
    w_out,
    mlp_gain,
    w_gate,
    w_up,
    w_down,
):
    full_width = tokens.shape[1] * lax.axis_size(KV) * lax.axis_size(TP)
    kv_index = lax.axis_index(KV)
    tp_index = lax.axis_index(TP)
    row_block, square_total = spread_rows(tokens, attn_gain)
    block_rows = row_block.shape[1]
    forget_rows = lax.dynamic_slice_in_dim(w_forget, kv_index * block_rows, block_rows, 0)
    query_part = jnp.dot(row_block, w_query, preferred_element_type=jnp.float32)
    key_part = jnp.dot(row_block, w_key, preferred_element_type=jnp.float32)
    value_part = jnp.dot(row_block, w_value, preferred_element_type=jnp.float32)
    forget_part = jnp.dot(row_block, forget_rows, preferred_element_type=jnp.float32)
    query_sum, key_sum, value_sum, forget_sum, square_total = (
        by_axis(query_part, KV),
        by_axis(key_part, KV),
        by_axis(value_part, KV),
        by_axis(forget_part, KV),
        by_axis(square_total, KV),
    )
    first_rms = lax.rsqrt(square_total / full_width + epsilon)[:, None]
    query_local = (query_sum * first_rms).astype(jnp.bfloat16)
    key_new = (key_sum * first_rms).astype(jnp.bfloat16)
    value_new = (value_sum * first_rms).astype(jnp.bfloat16)
    log_gate = jax.nn.log_sigmoid(forget_sum * first_rms + forget_bias)
    query_all = collect(query_local, TP, 1)
    batch_rows, key_dims, span = cache_keys.shape
    groups = QUERY_HEAD_COUNT // KV_HEADS
    score_scale = HD ** (-0.5)
    query_grouped = query_all.reshape(batch_rows, KV_HEADS, groups, HD)
    keys_grouped = cache_keys.reshape(batch_rows, KV_HEADS, HD, span)
    values_grouped = cache_values.reshape(batch_rows, KV_HEADS, HD, span)
    scores = jnp.einsum(
        "bkgd,bkdj->bkgj", query_grouped, keys_grouped, preferred_element_type=jnp.float32
    ).reshape(batch_rows, QUERY_HEAD_COUNT, span)
    scores = scores * score_scale + cache_decay + log_gate[:, :, None]
    first_slot = (kv_index * lax.axis_size(TP) + tp_index) * span
    token_positions = first_slot + lax.iota(jnp.int32, span)
    is_live = (token_positions[None, :] < lengths[:, None])[:, None, :]
    scores = jnp.where(is_live, scores, masked_score)
    own_score = (
        jnp.einsum(
            "inpo,ino->inp",
            query_grouped,
            key_new.reshape(batch_rows, KV_HEADS, HD),
            preferred_element_type=jnp.float32,
        ).reshape(batch_rows, QUERY_HEAD_COUNT)
        * score_scale
    )
    local_top = jnp.maximum(jnp.max(scores, axis=2), own_score)
    head_count = w_out.shape[0] // HD
    head_start = tp_index * head_count
    weights = jnp.where(is_live, jnp.exp(scores - local_top[:, :, None]), 0.0)
    weight_total = jnp.sum(weights, axis=2)
    rounded = weights.astype(jnp.bfloat16).reshape(batch_rows, KV_HEADS, groups, span)
    value_sums = jnp.einsum(
        "bkgj,bkdj->bkgd", rounded, values_grouped, preferred_element_type=jnp.float32
    ).reshape(batch_rows, QUERY_HEAD_COUNT, HD)
    weight_total, value_sums = (weight_total, value_sums)
    score_top, weight_total, value_sums = merged_by_axis(
        (local_top, weight_total, value_sums), KV_TP, combine_partials
    )
    weight_total = lax.dynamic_slice_in_dim(weight_total, head_start, head_count, 1)
    value_sums = lax.dynamic_slice_in_dim(value_sums, head_start, head_count, 1)
    score_top = lax.dynamic_slice_in_dim(score_top, head_start, head_count, 1)
    own_here = lax.dynamic_slice_in_dim(own_score, head_start, head_count, 1)
    new_values = jnp.repeat(value_new.reshape(batch_rows, KV_HEADS, HD), groups, axis=1)
    new_values = lax.dynamic_slice_in_dim(new_values, head_start, head_count, 1).astype(jnp.float32)
    own_weight = jnp.exp(own_here - score_top)
    heads_out = (value_sums + own_weight[:, :, None] * new_values) / (weight_total + own_weight)[
        :, :, None
    ]
    head_gains = lax.dynamic_slice_in_dim(out_gain, head_start * HD, head_count * HD, 0).reshape(
        head_count, HD
    )
    normed = (
        heads_out
        * lax.rsqrt(jnp.mean(jnp.square(heads_out), axis=2, keepdims=True) + epsilon)
        * head_gains
    )
    normed = normed.astype(jnp.bfloat16).reshape(batch_rows, head_count * HD)
    attn_part = jnp.dot(normed, w_out, preferred_element_type=jnp.float32)
    attn_share = summed_on_arrival(attn_part, TP, 1)
    residual = (tokens.astype(jnp.float32) + attn_share).astype(jnp.bfloat16)
    mlp_block, mlp_squares = spread_rows(residual, mlp_gain)
    gate_part = jnp.dot(mlp_block, w_gate, preferred_element_type=jnp.float32)
    up_part = jnp.dot(mlp_block, w_up, preferred_element_type=jnp.float32)
    gate_sum, up_sum, mlp_squares = (
        by_axis(gate_part, KV),
        by_axis(up_part, KV),
        by_axis(mlp_squares, KV),
    )
    second_rms = lax.rsqrt(mlp_squares / full_width + epsilon)[:, None]
    hidden = (jax.nn.silu(gate_sum * second_rms) * (up_sum * second_rms)).astype(jnp.bfloat16)
    down_part = jnp.dot(hidden, w_down, preferred_element_type=jnp.float32)
    mlp_share = summed_on_arrival(down_part, TP, 1)
    return (residual.astype(jnp.float32) + mlp_share).astype(jnp.bfloat16)


def solution(mesh):
    torus = Mesh(mesh.devices.reshape(4, 4, 16, 2), ("kv_0", "kv_1", "tp_0", "tp_1"))
    placed = (
        P(None, KV_TP),
        P(),
        P(KV_TP),
        P(KV, TP),
        P(KV, None),
        P(KV, None),
        P(),
        P(),
        P(None, None, KV_TP),
        P(None, None, KV_TP),
        P(None, None, KV_TP),
        P(),
        P(TP, KV),
        P(KV_TP),
        P(KV, TP),
        P(KV, TP),
        P(TP, KV),
    )
    return jax.shard_map(
        body, mesh=torus, in_specs=placed, out_specs=P(None, KV_TP), check_vma=False
    )
```

profile of v0, /device:TPU:1, one launch (start us, length us, event | category | flops | bytes accessed | tf_op | source)
XLA Modules:
  0.0 252.3 jit_solution(7297757308476043918)
XLA Ops:
  0.0 0.8 copy.80
  0.9 0.6 broadcast_in_dim.32
  1.5 16.7 %all-to-all-start.1 = ((f32[32,3,1]{1,2,0:T(1,128)}), f32[32,3,1]{1,2,0:T(1,128)S(1)}, u32[]{:S(2)}, u32[]{:S(2)}) async-start(f32[32,3,1]{1,2,0:T(1,128)} %broadcast_in_dim.32), calls=%async_computation.1 | async-start | bytes 32768 | tf_op jit(solution)/shard_map/all_to_all | solution.py:19
  18.4 11.6 %all-to-all-done.1 = f32[32,3,1]{1,2,0:T(1,128)S(1)} async-done(((f32[32,3,1]{1,2,0:T(1,128)}), f32[32,3,1]{1,2,0:T(1,128)S(1)}, u32[]{:S(2)}, u32[]{:S(2)}) %all-to-all-start.1) | async-done | bytes 416 | tf_op jit(solution)/shard_map/all_to_all | solution.py:19
  30.0 0.6 broadcast_in_dim.31
  30.6 4.6 %all-to-all-start = ((bf16[32,3,8]{2,1,0:T(4,128)(2,1)}), bf16[32,3,8]{2,1,0:T(4,128)(2,1)S(1)}, u32[]{:S(2)}, u32[]{:S(2)}) async-start(bf16[32,3,8]{2,1,0:T(4,128)(2,1)} %broadcast_in_dim.31), calls=%async_computation | async-start | bytes 65536 | tf_op jit(solution)/shard_map/all_to_all | solution.py:19
  35.4 0.8 dynamic_slice.27
  36.2 11.2 %all-to-all-done = bf16[32,3,8]{2,1,0:T(4,128)(2,1)S(1)} async-done(((bf16[32,3,8]{2,1,0:T(4,128)(2,1)}), bf16[32,3,8]{2,1,0:T(4,128)(2,1)S(1)}, u32[]{:S(2)}, u32[]{:S(2)}) %all-to-all-start) | async-done | bytes 1568 | tf_op jit(solution)/shard_map/all_to_all | solution.py:19
  47.7 0.1 fusion.201
  47.8 0.5 copy-done.7
  48.3 0.1 fusion.204
  48.6 8.9 %all-reduce.11 = (f32[3,128]{1,0:T(4,128)S(1)}, f32[3]{0:T(128)S(1)}, f32[3,64]{1,0:T(4,128)S(1)}, f32[3,32]{1,0:T(4,128)S(1)}, f32[3,128]{1,0:T(4,128)S(1)}) all-reduce(f32[3,128]{1,0:T(4,128)S(1)} %fusion.204, f32[3]{0:T(128)S(1)} %reduce_sum.73, ...), channel_id=1, replica_groups=mesh['kv_0'=4,'kv_1'=4,'tp_0'=16,'tp_1'=2] {'kv_0'}, use_global_device_ids=true, to_apply=%region_12.13 | all-reduce | flops 1059 | bytes 8472 | tf_op jit(solution)/shard_map/psum | solution.py:35
  57.5 8.7 %all-reduce.9 = (f32[3,128]{1,0:T(4,128)S(1)}, f32[3]{0:T(128)S(1)}, f32[3,64]{1,0:T(4,128)S(1)}, f32[3,32]{1,0:T(4,128)S(1)}, f32[3,128]{1,0:T(4,128)S(1)}) all-reduce(f32[3,128]{1,0:T(4,128)S(1)} %get-tuple-element.22, f32[3]{0:T(128)S(1)} %get-tuple-element.23, ...), channel_id=1, replica_groups=mesh['kv_0'=4,'kv_1'=4,'tp_0'=16,'tp_1'=2] {'kv_1'}, use_global_device_ids=true, to_apply=%region_13.14 | all-reduce | flops 1059 | bytes 8472 | tf_op jit(solution)/shard_map/psum | solution.py:35
  66.3 0.6 broadcast_in_dim.33
  66.9 8.6 %all-to-all-start.2 = ((bf16[32,3,64]{2,1,0:T(4,128)(2,1)}), bf16[32,3,64]{2,1,0:T(4,128)(2,1)S(1)}, u32[]{:S(2)}, u32[]{:S(2)}) async-start(bf16[32,3,64]{2,1,0:T(4,128)(2,1)} %broadcast_in_dim.33), calls=%async_computation.2 | async-start | bytes 65536 | tf_op jit(solution)/shard_map/all_to_all | solution.py:19
  75.5 0.7 copy-done.12
  76.4 11.3 %all-to-all-done.2 = bf16[32,3,64]{2,1,0:T(4,128)(2,1)S(1)} async-done(((bf16[32,3,64]{2,1,0:T(4,128)(2,1)}), bf16[32,3,64]{2,1,0:T(4,128)(2,1)S(1)}, u32[]{:S(2)}, u32[]{:S(2)}) %all-to-all-start.2) | async-done | bytes 12320 | tf_op jit(solution)/shard_map/all_to_all | solution.py:19
  88.0 0.1 convolution_multiply_fusion
  88.2 0.8 copy-done.5
  89.2 0.2 fusion.2
  89.4 0.6 copy-done.2
  89.9 0.1 fusion.203
  90.8 9.1 %all-gather.4 = f32[4,100,64]{1,2,0:T(8,128)S(1)} all-gather(f32[1,100,64]{1,2,0:T(8,128)S(1)} %maximum_bitcast_fusion), channel_id=2, replica_groups=mesh['kv_0'=4,'kv_1'=4,'tp_0'=16,'tp_1'=2] {'kv_0'}, dimensions={0}, use_global_device_ids=true | all-gather | bytes 128000 | tf_op jit(solution)/shard_map/all_gather | solution.py:47
  100.9 9.1 %all-gather.5 = f32[4,100,64]{1,2,0:T(8,128)S(1)} all-gather(f32[1,100,64]{1,2,0:T(8,128)S(1)} %maximum_bitcast_fusion.1), channel_id=3, replica_groups=mesh['kv_0'=4,'kv_1'=4,'tp_0'=16,'tp_1'=2] {'kv_1'}, dimensions={0}, use_global_device_ids=true | all-gather | bytes 128000 | tf_op jit(solution)/shard_map/all_gather | solution.py:47
  110.0 0.1 fusion.196
  111.0 22.9 %all-gather.6 = f32[16,100,64]{1,2,0:T(8,128)S(1)} all-gather(f32[1,100,64]{1,2,0:T(8,128)S(1)} %maximum_bitcast_fusion.2), channel_id=4, replica_groups=mesh['kv_0'=4,'kv_1'=4,'tp_0'=16,'tp_1'=2] {'tp_0'}, dimensions={0}, use_global_device_ids=true | all-gather | bytes 435200 | tf_op jit(solution)/shard_map/all_gather | solution.py:47
  133.9 0.3 fusion.195
  134.2 0.2 copy.95
  134.6 0.2 copy.96
  135.5 15.0 %all-gather.7 = f32[2,100,64]{1,2,0:T(8,128)S(1)} all-gather(f32[1,100,64]{1,2,0:T(8,128)S(1)} %maximum_bitcast_fusion.3), channel_id=5, replica_groups=mesh['kv_0'=4,'kv_1'=4,'tp_0'=16,'tp_1'=2] {'tp_1'}, dimensions={0}, use_global_device_ids=true | all-gather | bytes 76800 | tf_op jit(solution)/shard_map/all_gather | solution.py:47
  151.7 0.2 fusion.177
  151.9 0.2 multiply_reduce_fusion
  152.2 0.2 convolution_bitcast_fusion
  152.3 0.1 copy.105
  152.5 17.7 %all_to_all.35 = f32[32,3,8]{2,1,0:T(4,128)S(1)} all-to-all(f32[32,3,8]{2,1,0:T(4,128)S(1)} %copy.105), channel_id=1, replica_groups=mesh['kv_0'=4,'kv_1'=4,'tp_0'=16,'tp_1'=2] {'tp_0','tp_1'}, dimensions={0} | all-to-all | bytes 6144 | tf_op jit(solution)/shard_map/all_to_all | solution.py:73
  170.4 0.6 broadcast_in_dim.38
  171.0 5.1 %all-to-all-start.5 = ((f32[32,3,1]{1,2,0:T(1,128)}), f32[32,3,1]{1,2,0:T(1,128)S(1)}, u32[]{:S(2)}, u32[]{:S(2)}) async-start(f32[32,3,1]{1,2,0:T(1,128)} %broadcast_in_dim.38), calls=%async_computation.5 | async-start | bytes 32768 | tf_op jit(solution)/shard_map/all_to_all | solution.py:19
  176.3 11.7 %all-to-all-done.5 = f32[32,3,1]{1,2,0:T(1,128)S(1)} async-done(((f32[32,3,1]{1,2,0:T(1,128)}), f32[32,3,1]{1,2,0:T(1,128)S(1)}, u32[]{:S(2)}, u32[]{:S(2)}) %all-to-all-start.5) | async-done | bytes 416 | tf_op jit(solution)/shard_map/all_to_all | solution.py:19
  188.0 0.6 broadcast_in_dim.37
  188.6 4.5 %all-to-all-start.4 = ((bf16[32,3,8]{2,1,0:T(4,128)(2,1)}), bf16[32,3,8]{2,1,0:T(4,128)(2,1)S(1)}, u32[]{:S(2)}, u32[]{:S(2)}) async-start(bf16[32,3,8]{2,1,0:T(4,128)(2,1)} %broadcast_in_dim.37), calls=%async_computation.4 | async-start | bytes 65536 | tf_op jit(solution)/shard_map/all_to_all | solution.py:19
  193.2 12.2 %all-to-all-done.4 = bf16[32,3,8]{2,1,0:T(4,128)(2,1)S(1)} async-done(((bf16[32,3,8]{2,1,0:T(4,128)(2,1)}), bf16[32,3,8]{2,1,0:T(4,128)(2,1)S(1)}, u32[]{:S(2)}, u32[]{:S(2)}) %all-to-all-start.4) | async-done | bytes 1568 | tf_op jit(solution)/shard_map/all_to_all | solution.py:19
  205.5 0.1 fusion.205
  205.7 0.2 fusion.206
  205.8 10.8 %all-reduce.10 = (f32[3,352]{1,0:T(4,128)S(1)}, f32[3,352]{1,0:T(4,128)S(1)}, f32[3]{0:T(128)S(1)}) all-reduce(f32[3,352]{1,0:T(4,128)S(1)} %fusion.206, f32[3,352]{1,0:T(4,128)S(1)} %fusion.205, f32[3]{0:T(128)S(1)} %reduce_sum.78), channel_id=1, replica_groups=mesh['kv_0'=4,'kv_1'=4,'tp_0'=16,'tp_1'=2] {'kv_0'}, use_global_device_ids=true, to_apply=%region_22.23 | all-reduce | flops 2115 | bytes 16920 | tf_op jit(solution)/shard_map/psum | solution.py:35
  216.7 11.1 %all-reduce.8 = (f32[3,352]{1,0:T(4,128)S(1)}, f32[3,352]{1,0:T(4,128)S(1)}, f32[3]{0:T(128)S(1)}) all-reduce(f32[3,352]{1,0:T(4,128)S(1)} %get-tuple-element.19, f32[3,352]{1,0:T(4,128)S(1)} %get-tuple-element.20, f32[3]{0:T(128)S(1)} %get-tuple-element.21), channel_id=1, replica_groups=mesh['kv_0'=4,'kv_1'=4,'tp_0'=16,'tp_1'=2] {'kv_1'}, use_global_device_ids=true, to_apply=%region_23.24 | all-reduce | flops 2115 | bytes 16920 | tf_op jit(solution)/shard_map/psum | solution.py:35
  227.8 0.2 fusion.77
  228.2 23.3 %all_to_all.36 = f32[32,3,8]{2,1,0:T(4,128)S(1)} all-to-all(f32[32,3,8]{2,1,0:T(4,128)S(1)} %copy.109), channel_id=1, replica_groups=mesh['kv_0'=4,'kv_1'=4,'tp_0'=16,'tp_1'=2] {'tp_0','tp_1'}, dimensions={0} | all-to-all | bytes 6144 | tf_op jit(solution)/shard_map/all_to_all | solution.py:73
  251.7 0.7 copy.111
  (133 shorter events, 7.0 us)
Async XLA Ops:
  0.0 48.4 %copy-start = (bf16[4096,32]{0,1:T(8,128)(2,1)S(1)}, bf16[4096,32]{0,1:T(8,128)(2,1)}, u32[]{:S(2)}) copy-start(bf16[4096,32]{0,1:T(8,128)(2,1)} %param.23) | copy-start | bytes 786436
  0.0 0.8 copy-start.10
  1.5 28.5 %all-to-all-start.1 = ((f32[32,3,1]{1,2,0:T(1,128)}), f32[32,3,1]{1,2,0:T(1,128)S(1)}, u32[]{:S(2)}, u32[]{:S(2)}) async-start(f32[32,3,1]{1,2,0:T(1,128)} %broadcast_in_dim.32), calls=%async_computation.1 | async-start | bytes 32768 | tf_op jit(solution)/shard_map/all_to_all | solution.py:19
  30.6 4.6 %copy-start.11 = (s32[3]{0:T(128)S(1)}, s32[3]{0:T(128)}, u32[]{:S(2)}) copy-start(s32[3]{0:T(128)} %param.18) | copy-start | bytes 40
  30.6 4.7 %copy-start.8 = (bf16[64,256]{1,0:T(8,128)(2,1)S(1)}, bf16[64,256]{1,0:T(8,128)(2,1)}, u32[]{:S(2)}) copy-start(bf16[64,256]{1,0:T(8,128)(2,1)} %param.29) | copy-start | bytes 98308
  30.6 16.8 %all-to-all-start = ((bf16[32,3,8]{2,1,0:T(4,128)(2,1)}), bf16[32,3,8]{2,1,0:T(4,128)(2,1)S(1)}, u32[]{:S(2)}, u32[]{:S(2)}) async-start(bf16[32,3,8]{2,1,0:T(4,128)(2,1)} %broadcast_in_dim.31), calls=%async_computation | async-start | bytes 65536 | tf_op jit(solution)/shard_map/all_to_all | solution.py:19
  36.2 11.4 %copy-start.9 = (bf16[256,64]{0,1:T(8,128)(2,1)S(1)}, bf16[256,64]{0,1:T(8,128)(2,1)}, u32[]{:S(2)}) copy-start(bf16[256,64]{0,1:T(8,128)(2,1)} %param.20) | copy-start | bytes 98308
  36.2 11.5 %copy-start.6 = (bf16[256,128]{1,0:T(8,128)(2,1)S(1)}, bf16[256,128]{1,0:T(8,128)(2,1)}, u32[]{:S(2)}) copy-start(bf16[256,128]{1,0:T(8,128)(2,1)} %param.21) | copy-start | bytes 196612
  47.5 0.8 copy-start.7
  48.3 39.7 %copy-start.1 = (bf16[3,128,256]{2,1,0:T(8,128)(2,1)S(1)}, bf16[3,128,256]{2,1,0:T(8,128)(2,1)}, u32[]{:S(2)}) copy-start(bf16[3,128,256]{2,1,0:T(8,128)(2,1)} %param.25) | copy-start | bytes 589828
  66.9 20.8 %all-to-all-start.2 = ((bf16[32,3,64]{2,1,0:T(4,128)(2,1)}), bf16[32,3,64]{2,1,0:T(4,128)(2,1)S(1)}, u32[]{:S(2)}, u32[]{:S(2)}) async-start(bf16[32,3,64]{2,1,0:T(4,128)(2,1)} %broadcast_in_dim.33), calls=%async_computation.2 | async-start | bytes 65536 | tf_op jit(solution)/shard_map/all_to_all | solution.py:19
  75.5 0.7 copy-start.12
  88.0 0.9 copy-start.5
  89.0 0.9 copy-start.2
  152.5 23.6 %copy-start.13 = (f32[8]{0:T(128)S(1)}, f32[8]{0:T(128)}, u32[]{:S(2)}) copy-start(f32[8]{0:T(128)} %param.30) | copy-start | bytes 100
  170.2 35.3 %copy-start.3 = (bf16[256,352]{0,1:T(8,128)(2,1)S(1)}, bf16[256,352]{0,1:T(8,128)(2,1)}, u32[]{:S(2)}) copy-start(bf16[256,352]{0,1:T(8,128)(2,1)} %param.31) | copy-start | bytes 540676
  171.0 17.0 %all-to-all-start.5 = ((f32[32,3,1]{1,2,0:T(1,128)}), f32[32,3,1]{1,2,0:T(1,128)S(1)}, u32[]{:S(2)}, u32[]{:S(2)}) async-start(f32[32,3,1]{1,2,0:T(1,128)} %broadcast_in_dim.38), calls=%async_computation.5 | async-start | bytes 32768 | tf_op jit(solution)/shard_map/all_to_all | solution.py:19
  188.6 17.0 %copy-start.4 = (bf16[256,352]{0,1:T(8,128)(2,1)S(1)}, bf16[256,352]{0,1:T(8,128)(2,1)}, u32[]{:S(2)}) copy-start(bf16[256,352]{0,1:T(8,128)(2,1)} %param.32) | copy-start | bytes 540676
  188.6 16.8 %all-to-all-start.4 = ((bf16[32,3,8]{2,1,0:T(4,128)(2,1)}), bf16[32,3,8]{2,1,0:T(4,128)(2,1)S(1)}, u32[]{:S(2)}, u32[]{:S(2)}) async-start(bf16[32,3,8]{2,1,0:T(4,128)(2,1)} %broadcast_in_dim.37), calls=%async_computation.4 | async-start | bytes 65536 | tf_op jit(solution)/shard_map/all_to_all | solution.py:19
  205.5 22.3 %copy-start.14 = (bf16[352,256]{1,0:T(8,128)(2,1)S(1)}, bf16[352,256]{1,0:T(8,128)(2,1)}, u32[]{:S(2)}) copy-start(bf16[352,256]{1,0:T(8,128)(2,1)} %param.33) | copy-start | bytes 540676
where the time goes:
time: 253 us; the launch traced here: 252 us
  blocking collectives  137 us (54%)
  waiting for transfers between devices  58.1 us (23%)
  starting transfers between devices  39.5 us (16%)
  local copies, waits for them, and re-layouts  13.8 us (5%)
    all_to_all x5, waiting for transfers between devices, sent_to_all(): return lax.all_to_all(copies, axis, split_axis=0, concat_axis=0, tiled=True)  58.1 us
    all_gather x4, blocking collectives, all_in_one(): both, at, found = (lax.all_gather(jnp.concatenate(lines), axis), 0, {})  56.1 us
    all_to_all x2, blocking collectives, summed_on_arrival(): blocks = lax.all_to_all(in_blocks(x, dim, length), axis, 0, 0, tiled=True)  41.1 us
    psum x4, blocking collectives, by_axis(): x = lax.psum(x, axis)  39.6 us
    all_to_all x5, starting transfers between devices, sent_to_all(): return lax.all_to_all(copies, axis, split_axis=0, concat_axis=0, tiled=True)  39.5 us
  transfers between devices with their start and end apart: 5, of which 5 were waited for; matrix products, arithmetic and copies ran while one was open for 1% of the time, Pallas kernels for 0%

commit v1 on v0

--- a/solution.py
+++ b/solution.py
@@ -3,6 +3,7 @@
 from jax import lax
 from jax.sharding import Mesh
 from jax.sharding import PartitionSpec as P
+from jax.lax import all_gather
 
 QUERY_HEAD_COUNT = 32
 HD = 64
@@ -14,6 +15,10 @@
 masked_score = -1e30
 
 
+def fill_points(dev_axis, chunk):
+    return all_gather(chunk, dev_axis).sum(axis=0)
+
+
 def sent_to_all(x, axis):
     copies = jnp.broadcast_to(x, (lax.axis_size(axis), *x.shape))
     return lax.all_to_all(copies, axis, split_axis=0, concat_axis=0, tiled=True)
@@ -32,7 +37,7 @@
 
 def by_axis(x, axes):
     for axis in axes:
-        x = lax.psum(x, axis)
+        x = fill_points(axis, x)
     return x
 
 

time: 253 us -> 361 us (1.43)
  blocking collectives: 137 us -> 254 us
  waiting for transfers between devices: 58.1 us -> 24.3 us
  starting transfers between devices: 39.5 us -> 58.4 us
  local copies, waits for them, and re-layouts: 13.8 us -> 17.8 us
    all_gather x0 -> x12, blocking collectives: none -> 102 us  [fill_points(): return all_gather(chunk, dev_axis).sum(axis=0)]
    psum x4 -> x0, blocking collectives: 39.6 us -> none  [by_axis(): x = lax.psum(x, axis)]
    all_to_all x5, waiting for transfers between devices: 58.1 us -> 24.3 us  [sent_to_all(): return lax.all_to_all(copies, axis, split_axis=0, concat_axis=0, tiled=True)]
    unnamed x0 -> x4, blocking collectives: none -> 30.3 us
    all_to_all x5, starting transfers between devices: 39.5 us -> 58.4 us  [sent_to_all(): return lax.all_to_all(copies, axis, split_axis=0, concat_axis=0, tiled=True)]
    all_to_all x2, blocking collectives: 41.1 us -> 54.5 us  [summed_on_arrival(): blocks = lax.all_to_all(in_blocks(x, dim, length), axis, 0, 0, tiled=True)]
    all_gather x4, blocking collectives: 56.1 us -> 67.5 us  [all_in_one(): both, at, found = (lax.all_gather(jnp.concatenate(lines), axis), 0, {})]
    unnamed x35 -> x45, local copies, waits for them, and re-layouts: 3.67 us -> 7.26 us
  transfers between devices with their start and end apart: 5 -> 5, of which waited for: 5 -> 3; matrix products, arithmetic and copies ran while one was open for 1% -> 1% of each run, Pallas kernels for 0% -> 0%
where the time goes in v1:
time: 361 us; the launch traced here: 360 us
  blocking collectives  254 us (70%)
  starting transfers between devices  58.4 us (16%)
  waiting for transfers between devices  24.3 us (7%)
  local copies, waits for them, and re-layouts  17.8 us (5%)
    all_gather x12, blocking collectives, fill_points(): return all_gather(chunk, dev_axis).sum(axis=0)  102 us
    all_gather x4, blocking collectives, all_in_one(): both, at, found = (lax.all_gather(jnp.concatenate(lines), axis), 0, {})  67.5 us
    all_to_all x5, starting transfers between devices, sent_to_all(): return lax.all_to_all(copies, axis, split_axis=0, concat_axis=0, tiled=True)  58.4 us
    all_to_all x2, blocking collectives, summed_on_arrival(): blocks = lax.all_to_all(in_blocks(x, dim, length), axis, 0, 0, tiled=True)  54.5 us
    unnamed x4, blocking collectives  30.3 us
    all_to_all x5, waiting for transfers between devices, sent_to_all(): return lax.all_to_all(copies, axis, split_axis=0, concat_axis=0, tiled=True)  24.3 us
    unnamed x45, local copies, waits for them, and re-layouts  7.26 us
  transfers between devices with their start and end apart: 5, of which 3 were waited for; matrix products, arithmetic and copies ran while one was open for 1% of the time, Pallas kernels for 0%

profile of v1, /device:TPU:1, one launch (start us, length us, event | category | flops | bytes accessed | tf_op | source)
XLA Modules:
  0.0 360.2 jit_solution(9235992510378750839)
XLA Ops:
  0.0 0.8 copy.79
  0.9 0.6 broadcast_in_dim.32
  1.5 16.7 %all-to-all-start.1 = ((f32[32,3,1]{1,2,0:T(1,128)}), f32[32,3,1]{1,2,0:T(1,128)S(1)}, u32[]{:S(2)}, u32[]{:S(2)}) async-start(f32[32,3,1]{1,2,0:T(1,128)} %broadcast_in_dim.32), calls=%async_computation.1 | async-start | bytes 32768 | tf_op jit(solution)/shard_map/all_to_all | solution.py:24
  18.3 0.6 copy-done.11
  19.1 1.3 dynamic-slice
  20.4 1.3 dynamic-slice.1
  23.1 7.0 %all-to-all-done.1 = f32[32,3,1]{1,2,0:T(1,128)S(1)} async-done(((f32[32,3,1]{1,2,0:T(1,128)}), f32[32,3,1]{1,2,0:T(1,128)S(1)}, u32[]{:S(2)}, u32[]{:S(2)}) %all-to-all-start.1) | async-done | bytes 416 | tf_op jit(solution)/shard_map/all_to_all | solution.py:24
  30.0 0.6 broadcast_in_dim.31
  30.6 5.2 %all-to-all-start = ((bf16[32,3,8]{2,1,0:T(4,128)(2,1)}), bf16[32,3,8]{2,1,0:T(4,128)(2,1)S(1)}, u32[]{:S(2)}, u32[]{:S(2)}) async-start(bf16[32,3,8]{2,1,0:T(4,128)(2,1)} %broadcast_in_dim.31), calls=%async_computation | async-start | bytes 65536 | tf_op jit(solution)/shard_map/all_to_all | solution.py:24
  35.9 0.2 dynamic-update-slice
  36.2 9.3 %all-reduce.8 = f32[12]{0:T(128)S(1)} all-reduce(f32[12]{0:T(128)S(1)} %dynamic-update-slice), channel_id=4, replica_groups=mesh['kv_0'=4,'kv_1'=4,'tp_0'=16,'tp_1'=2] {'kv_0'}, use_global_device_ids=true, to_apply=%add.8 | all-reduce | flops 12 | bytes 96
  45.6 0.2 dynamic-update-slice.1
  45.8 0.8 dynamic_slice.27
  46.6 8.4 %all-reduce.9 = f32[12]{0:T(128)S(1)} all-reduce(f32[12]{0:T(128)S(1)} %dynamic-update-slice.1), channel_id=5, replica_groups=mesh['kv_0'=4,'kv_1'=4,'tp_0'=16,'tp_1'=2] {'kv_1'}, use_global_device_ids=true, to_apply=%add.9 | all-reduce | flops 12 | bytes 96
  55.4 8.1 %all-gather.22 = f32[4,3,32]{2,1,0:T(4,128)S(1)} all-gather(f32[1,3,32]{2,1,0:T(4,128)S(1)} %convolution_bitcast_fusion.5), channel_id=6, replica_groups=mesh['kv_0'=4,'kv_1'=4,'tp_0'=16,'tp_1'=2] {'kv_0'}, dimensions={0}, use_global_device_ids=true | all-gather | bytes 1920 | tf_op jit(solution)/shard_map/all_gather | solution.py:19
  63.5 8.1 %all-gather.23 = f32[4,3,32]{2,1,0:T(4,128)S(1)} all-gather(f32[1,3,32]{2,1,0:T(4,128)S(1)} %bitcast.777), channel_id=7, replica_groups=mesh['kv_0'=4,'kv_1'=4,'tp_0'=16,'tp_1'=2] {'kv_1'}, dimensions={0}, use_global_device_ids=true | all-gather | bytes 1920 | tf_op jit(solution)/shard_map/all_gather | solution.py:19
  71.8 8.1 %all-gather.20 = f32[4,3,64]{2,1,0:T(4,128)S(1)} all-gather(f32[1,3,64]{2,1,0:T(4,128)S(1)} %convolution_bitcast_fusion.6), channel_id=2, replica_groups=mesh['kv_0'=4,'kv_1'=4,'tp_0'=16,'tp_1'=2] {'kv_0'}, dimensions={0}, use_global_device_ids=true | all-gather | bytes 3840 | tf_op jit(solution)/shard_map/all_gather | solution.py:19
  80.0 8.3 %all-gather.21 = f32[4,3,64]{2,1,0:T(4,128)S(1)} all-gather(f32[1,3,64]{2,1,0:T(4,128)S(1)} %bitcast.778), channel_id=3, replica_groups=mesh['kv_0'=4,'kv_1'=4,'tp_0'=16,'tp_1'=2] {'kv_1'}, dimensions={0}, use_global_device_ids=true | all-gather | bytes 3840 | tf_op jit(solution)/shard_map/all_gather | solution.py:19
  88.3 0.6 broadcast_in_dim.33
  88.9 25.2 %all-to-all-start.2 = ((bf16[32,3,64]{2,1,0:T(4,128)(2,1)}), bf16[32,3,64]{2,1,0:T(4,128)(2,1)S(1)}, u32[]{:S(2)}, u32[]{:S(2)}) async-start(bf16[32,3,64]{2,1,0:T(4,128)(2,1)} %broadcast_in_dim.33), calls=%async_computation.2 | async-start | bytes 65536 | tf_op jit(solution)/shard_map/all_to_all | solution.py:24
  114.3 8.1 %all-gather.24 = f32[4,3,128]{2,1,0:T(4,128)S(1)} all-gather(f32[1,3,128]{2,1,0:T(4,128)S(1)} %convolution_bitcast_fusion.4), channel_id=8, replica_groups=mesh['kv_0'=4,'kv_1'=4,'tp_0'=16,'tp_1'=2] {'kv_0'}, dimensions={0}, use_global_device_ids=true | all-gather | bytes 7680 | tf_op jit(solution)/shard_map/all_gather | solution.py:19
  122.5 8.1 %all-gather.25 = f32[4,3,128]{2,1,0:T(4,128)S(1)} all-gather(f32[1,3,128]{2,1,0:T(4,128)S(1)} %bitcast.779), channel_id=9, replica_groups=mesh['kv_0'=4,'kv_1'=4,'tp_0'=16,'tp_1'=2] {'kv_1'}, dimensions={0}, use_global_device_ids=true | all-gather | bytes 7680 | tf_op jit(solution)/shard_map/all_gather | solution.py:19
  130.8 8.1 %all-gather.30 = f32[4,3,128]{2,1,0:T(4,128)S(1)} all-gather(f32[1,3,128]{2,1,0:T(4,128)S(1)} %convolution_bitcast_fusion.3), channel_id=14, replica_groups=mesh['kv_0'=4,'kv_1'=4,'tp_0'=16,'tp_1'=2] {'kv_0'}, dimensions={0}, use_global_device_ids=true | all-gather | bytes 7680 | tf_op jit(solution)/shard_map/all_gather | solution.py:19
  139.0 8.1 %all-gather.31 = f32[4,3,128]{2,1,0:T(4,128)S(1)} all-gather(f32[1,3,128]{2,1,0:T(4,128)S(1)} %bitcast.780), channel_id=15, replica_groups=mesh['kv_0'=4,'kv_1'=4,'tp_0'=16,'tp_1'=2] {'kv_1'}, dimensions={0}, use_global_device_ids=true | all-gather | bytes 7680 | tf_op jit(solution)/shard_map/all_gather | solution.py:19
  147.3 0.6 copy-done.12
  148.4 0.8 copy-done.5
  149.7 0.6 copy-done.2
  151.0 9.1 %all-gather.26 = f32[4,100,64]{1,2,0:T(8,128)S(1)} all-gather(f32[1,100,64]{1,2,0:T(8,128)S(1)} %maximum_bitcast_fusion), channel_id=10, replica_groups=mesh['kv_0'=4,'kv_1'=4,'tp_0'=16,'tp_1'=2] {'kv_0'}, dimensions={0}, use_global_device_ids=true | all-gather | bytes 128000 | tf_op jit(solution)/shard_map/all_gather | solution.py:52
  161.2 9.4 %all-gather.27 = f32[4,100,64]{1,2,0:T(8,128)S(1)} all-gather(f32[1,100,64]{1,2,0:T(8,128)S(1)} %maximum_bitcast_fusion.1), channel_id=11, replica_groups=mesh['kv_0'=4,'kv_1'=4,'tp_0'=16,'tp_1'=2] {'kv_1'}, dimensions={0}, use_global_device_ids=true | all-gather | bytes 128000 | tf_op jit(solution)/shard_map/all_gather | solution.py:52
  171.6 25.9 %all-gather.28 = f32[16,100,64]{1,2,0:T(8,128)S(1)} all-gather(f32[1,100,64]{1,2,0:T(8,128)S(1)} %maximum_bitcast_fusion.2), channel_id=12, replica_groups=mesh['kv_0'=4,'kv_1'=4,'tp_0'=16,'tp_1'=2] {'tp_0'}, dimensions={0}, use_global_device_ids=true | all-gather | bytes 435200 | tf_op jit(solution)/shard_map/all_gather | solution.py:52
  197.5 0.3 fusion.197
  199.0 23.1 %all-gather.29 = f32[2,100,64]{1,2,0:T(8,128)S(1)} all-gather(f32[1,100,64]{1,2,0:T(8,128)S(1)} %maximum_bitcast_fusion.3), channel_id=13, replica_groups=mesh['kv_0'=4,'kv_1'=4,'tp_0'=16,'tp_1'=2] {'tp_1'}, dimensions={0}, use_global_device_ids=true | all-gather | bytes 76800 | tf_op jit(solution)/shard_map/all_gather | solution.py:52
  224.1 22.4 %all_to_all.35 = f32[32,3,8]{2,1,0:T(4,128)S(1)} all-to-all(f32[32,3,8]{2,1,0:T(4,128)S(1)} %copy.104), channel_id=1, replica_groups=mesh['kv_0'=4,'kv_1'=4,'tp_0'=16,'tp_1'=2] {'tp_0','tp_1'}, dimensions={0} | all-to-all | bytes 6144 | tf_op jit(solution)/shard_map/all_to_all | solution.py:78
  246.6 0.6 broadcast_in_dim.38
  247.2 5.1 %all-to-all-start.5 = ((f32[32,3,1]{1,2,0:T(1,128)}), f32[32,3,1]{1,2,0:T(1,128)S(1)}, u32[]{:S(2)}, u32[]{:S(2)}) async-start(f32[32,3,1]{1,2,0:T(1,128)} %broadcast_in_dim.38), calls=%async_computation.5 | async-start | bytes 32768 | tf_op jit(solution)/shard_map/all_to_all | solution.py:24
  252.4 11.8 %all-to-all-done.5 = f32[32,3,1]{1,2,0:T(1,128)S(1)} async-done(((f32[32,3,1]{1,2,0:T(1,128)}), f32[32,3,1]{1,2,0:T(1,128)S(1)}, u32[]{:S(2)}, u32[]{:S(2)}) %all-to-all-start.5) | async-done | bytes 416 | tf_op jit(solution)/shard_map/all_to_all | solution.py:24
  264.7 6.0 %all-reduce.10 = f32[12]{0:T(128)S(1)} all-reduce(f32[12]{0:T(128)S(1)} %dynamic-update-slice.2), channel_id=18, replica_groups=mesh['kv_0'=4,'kv_1'=4,'tp_0'=16,'tp_1'=2] {'kv_0'}, use_global_device_ids=true, to_apply=%add.10 | all-reduce | flops 12 | bytes 96
  270.7 0.2 dynamic-update-slice.3
  271.0 0.6 broadcast_in_dim.37
  271.6 6.1 %all-to-all-start.4 = ((bf16[32,3,8]{2,1,0:T(4,128)(2,1)}), bf16[32,3,8]{2,1,0:T(4,128)(2,1)S(1)}, u32[]{:S(2)}, u32[]{:S(2)}) async-start(bf16[32,3,8]{2,1,0:T(4,128)(2,1)} %broadcast_in_dim.37), calls=%async_computation.4 | async-start | bytes 65536 | tf_op jit(solution)/shard_map/all_to_all | solution.py:24
  277.7 6.6 %all-reduce.11 = f32[12]{0:T(128)S(1)} all-reduce(f32[12]{0:T(128)S(1)} %dynamic-update-slice.3), channel_id=19, replica_groups=mesh['kv_0'=4,'kv_1'=4,'tp_0'=16,'tp_1'=2] {'kv_1'}, use_global_device_ids=true, to_apply=%add.11 | all-reduce | flops 12 | bytes 96
  284.4 5.5 %all-to-all-done.4 = bf16[32,3,8]{2,1,0:T(4,128)(2,1)S(1)} async-done(((bf16[32,3,8]{2,1,0:T(4,128)(2,1)}), bf16[32,3,8]{2,1,0:T(4,128)(2,1)S(1)}, u32[]{:S(2)}, u32[]{:S(2)}) %all-to-all-start.4) | async-done | bytes 1568 | tf_op jit(solution)/shard_map/all_to_all | solution.py:24
  290.2 9.1 %all-gather.32 = f32[4,3,352]{2,1,0:T(4,128)S(1)} all-gather(f32[1,3,352]{2,1,0:T(4,128)S(1)} %convolution_bitcast_fusion.2), channel_id=16, replica_groups=mesh['kv_0'=4,'kv_1'=4,'tp_0'=16,'tp_1'=2] {'kv_0'}, dimensions={0}, use_global_device_ids=true | all-gather | bytes 21120 | tf_op jit(solution)/shard_map/all_gather | solution.py:19
  299.3 9.1 %all-gather.33 = f32[4,3,352]{2,1,0:T(4,128)S(1)} all-gather(f32[1,3,352]{2,1,0:T(4,128)S(1)} %bitcast.775), channel_id=17, replica_groups=mesh['kv_0'=4,'kv_1'=4,'tp_0'=16,'tp_1'=2] {'kv_1'}, dimensions={0}, use_global_device_ids=true | all-gather | bytes 21120 | tf_op jit(solution)/shard_map/all_gather | solution.py:19
  308.6 9.1 %all-gather.34 = f32[4,3,352]{2,1,0:T(4,128)S(1)} all-gather(f32[1,3,352]{2,1,0:T(4,128)S(1)} %convolution_bitcast_fusion.1), channel_id=20, replica_groups=mesh['kv_0'=4,'kv_1'=4,'tp_0'=16,'tp_1'=2] {'kv_0'}, dimensions={0}, use_global_device_ids=true | all-gather | bytes 21120 | tf_op jit(solution)/shard_map/all_gather | solution.py:19
  317.7 9.2 %all-gather.35 = f32[4,3,352]{2,1,0:T(4,128)S(1)} all-gather(f32[1,3,352]{2,1,0:T(4,128)S(1)} %bitcast.776), channel_id=21, replica_groups=mesh['kv_0'=4,'kv_1'=4,'tp_0'=16,'tp_1'=2] {'kv_1'}, dimensions={0}, use_global_device_ids=true | all-gather | bytes 21120 | tf_op jit(solution)/shard_map/all_gather | solution.py:19
  327.3 32.1 %all_to_all.36 = f32[32,3,8]{2,1,0:T(4,128)S(1)} all-to-all(f32[32,3,8]{2,1,0:T(4,128)S(1)} %copy.108), channel_id=1, replica_groups=mesh['kv_0'=4,'kv_1'=4,'tp_0'=16,'tp_1'=2] {'tp_0','tp_1'}, dimensions={0} | all-to-all | bytes 6144 | tf_op jit(solution)/shard_map/all_to_all | solution.py:78
  359.6 0.7 copy.110
  (175 shorter events, 10.3 us)
Async XLA Ops:
  0.0 55.2 %copy-start = (bf16[4096,32]{0,1:T(8,128)(2,1)S(1)}, bf16[4096,32]{0,1:T(8,128)(2,1)}, u32[]{:S(2)}) copy-start(bf16[4096,32]{0,1:T(8,128)(2,1)} %param.23) | copy-start | bytes 786436
  0.0 0.8 copy-start.10
  1.5 28.5 %all-to-all-start.1 = ((f32[32,3,1]{1,2,0:T(1,128)}), f32[32,3,1]{1,2,0:T(1,128)S(1)}, u32[]{:S(2)}, u32[]{:S(2)}) async-start(f32[32,3,1]{1,2,0:T(1,128)} %broadcast_in_dim.32), calls=%async_computation.1 | async-start | bytes 32768 | tf_op jit(solution)/shard_map/all_to_all | solution.py:24
  18.3 0.7 copy-start.11
  18.3 4.7 %copy-start.8 = (bf16[64,256]{1,0:T(8,128)(2,1)S(1)}, bf16[64,256]{1,0:T(8,128)(2,1)}, u32[]{:S(2)}) copy-start(bf16[64,256]{1,0:T(8,128)(2,1)} %param.29) | copy-start | bytes 98308
  30.6 24.5 %all-to-all-start = ((bf16[32,3,8]{2,1,0:T(4,128)(2,1)}), bf16[32,3,8]{2,1,0:T(4,128)(2,1)S(1)}, u32[]{:S(2)}, u32[]{:S(2)}) async-start(bf16[32,3,8]{2,1,0:T(4,128)(2,1)} %broadcast_in_dim.31), calls=%async_computation | async-start | bytes 65536 | tf_op jit(solution)/shard_map/all_to_all | solution.py:24
  55.2 16.4 %copy-start.9 = (bf16[256,64]{0,1:T(8,128)(2,1)S(1)}, bf16[256,64]{0,1:T(8,128)(2,1)}, u32[]{:S(2)}) copy-start(bf16[256,64]{0,1:T(8,128)(2,1)} %param.20) | copy-start | bytes 98308
  79.9 34.2 %copy-start.6 = (bf16[256,128]{1,0:T(8,128)(2,1)S(1)}, bf16[256,128]{1,0:T(8,128)(2,1)}, u32[]{:S(2)}) copy-start(bf16[256,128]{1,0:T(8,128)(2,1)} %param.21) | copy-start | bytes 196612
  88.9 41.8 %copy-start.7 = (bf16[256,128]{1,0:T(8,128)(2,1)S(1)}, bf16[256,128]{1,0:T(8,128)(2,1)}, u32[]{:S(2)}) copy-start(bf16[256,128]{1,0:T(8,128)(2,1)} %param.22) | copy-start | bytes 196612
  88.9 59.0 %all-to-all-start.2 = ((bf16[32,3,64]{2,1,0:T(4,128)(2,1)}), bf16[32,3,64]{2,1,0:T(4,128)(2,1)S(1)}, u32[]{:S(2)}, u32[]{:S(2)}) async-start(bf16[32,3,64]{2,1,0:T(4,128)(2,1)} %broadcast_in_dim.33), calls=%async_computation.2 | async-start | bytes 65536 | tf_op jit(solution)/shard_map/all_to_all | solution.py:24
  114.2 34.1 %copy-start.1 = (bf16[3,128,256]{2,1,0:T(8,128)(2,1)S(1)}, bf16[3,128,256]{2,1,0:T(8,128)(2,1)}, u32[]{:S(2)}) copy-start(bf16[3,128,256]{2,1,0:T(8,128)(2,1)} %param.25) | copy-start | bytes 589828
  147.2 0.7 copy-start.12
  148.3 0.9 copy-start.5
  149.3 0.9 copy-start.2
  224.1 28.2 %copy-start.13 = (f32[8]{0:T(128)S(1)}, f32[8]{0:T(128)}, u32[]{:S(2)}) copy-start(f32[8]{0:T(128)} %param.30) | copy-start | bytes 100
  246.5 43.6 %copy-start.3 = (bf16[256,352]{0,1:T(8,128)(2,1)S(1)}, bf16[256,352]{0,1:T(8,128)(2,1)}, u32[]{:S(2)}) copy-start(bf16[256,352]{0,1:T(8,128)(2,1)} %param.31) | copy-start | bytes 540676
  247.2 17.0 %all-to-all-start.5 = ((f32[32,3,1]{1,2,0:T(1,128)}), f32[32,3,1]{1,2,0:T(1,128)S(1)}, u32[]{:S(2)}, u32[]{:S(2)}) async-start(f32[32,3,1]{1,2,0:T(1,128)} %broadcast_in_dim.38), calls=%async_computation.5 | async-start | bytes 32768 | tf_op jit(solution)/shard_map/all_to_all | solution.py:24
  271.6 18.4 %all-to-all-start.4 = ((bf16[32,3,8]{2,1,0:T(4,128)(2,1)}), bf16[32,3,8]{2,1,0:T(4,128)(2,1)S(1)}, u32[]{:S(2)}, u32[]{:S(2)}) async-start(bf16[32,3,8]{2,1,0:T(4,128)(2,1)} %broadcast_in_dim.37), calls=%async_computation.4 | async-start | bytes 65536 | tf_op jit(solution)/shard_map/all_to_all | solution.py:24
  290.0 18.5 %copy-start.4 = (bf16[256,352]{0,1:T(8,128)(2,1)S(1)}, bf16[256,352]{0,1:T(8,128)(2,1)}, u32[]{:S(2)}) copy-start(bf16[256,352]{0,1:T(8,128)(2,1)} %param.32) | copy-start | bytes 540676
  308.4 18.5 %copy-start.14 = (bf16[352,256]{1,0:T(8,128)(2,1)S(1)}, bf16[352,256]{1,0:T(8,128)(2,1)}, u32[]{:S(2)}) copy-start(bf16[352,256]{1,0:T(8,128)(2,1)} %param.33) | copy-start | bytes 540676
